TPU v7x, 32 devices: a whole 2x2x4 slice. The times are simulated.
32 devices in a mesh: ep: 4 (over y, x), tp: 8 (over z, core).
Axes of the slice: x: 2, y: 2, z: 4, core: 2. Of those that a mesh axis runs over, the one named last changes fastest.
Arguments:
- mix_query: bfloat16 [2048, 2048], P('ep', 'tp'), may hold values from -60 to 60
- mix_key: bfloat16 [2048, 2048], P('ep', 'tp'), may hold values from -60 to 60
- mix_value: bfloat16 [2048, 2048], P('ep', 'tp'), may hold values from -6 to 6
- head_lambda: float32 [16], P('tp'), may hold values from 0.3 to 0.8
- head_gain: float32 [128], replicated, may hold values from 0.1 to 1.9
- out_weight: bfloat16 [2048, 2048], P('tp'), may hold values from -0.125 to 0.125
- moe_input: bfloat16 [2048, 2048], P(('ep', 'tp')), may hold values from -6 to 6
- moe_gain: float32 [2048], replicated, may hold values from 0.1 to 1.9
- expert_ids: int32 [2048, 2], P(('ep', 'tp')), may hold values from 0 to 3, all different within a row; in each aligned block of 64 rows (0 to 63, 64 to 127, ...) at most 48 rows name the same one
- route_weight: float32 [2048, 2], P(('ep', 'tp')), may hold values from 0.2 to 1
- gate_weight: bfloat16 [4, 2048, 4096], P('ep', None, 'tp'), may hold values from -0.125 to 0.125
- up_weight: bfloat16 [4, 2048, 4096], P('ep', None, 'tp'), may hold values from -0.125 to 0.125
- down_weight: bfloat16 [4, 4096, 2048], P('ep', 'tp'), may hold values from -0.09375 to 0.09375
Outputs:
- mix_output: bfloat16 [2048, 2048], P(('ep', 'tp'))
- moe_output: bfloat16 [2048, 2048], P(('ep', 'tp'))
Inputs may be any that keep to these rules, and one draw needn't show every extreme that they name: `expert_ids`: in each aligned block of 64 rows (the rows of one device) no expert is named by more than 48 rows; a row names 2 different experts.
All inputs are finite; a program needn't handle non-finite values.
Results may differ from a plain program's by a relative error of at most 0.02.
The roundings to bfloat16 on the way count: a program that leaves them out, or rounds other values in their place, can miss the bound.
Values may be sent and summed in bfloat16 or wider, within the bound.
A program may use at most 128 MiB of HBM per device.

v0:
```python
import math

import jax
import jax.numpy as jnp
from jax import lax
from jax.experimental import pallas as pl
from jax.experimental.pallas import tpu as pltpu
from jax.sharding import PartitionSpec as P

epsilon = 1e-06
rotary_base = 10000.0
far_below = -1e30


def norm_rows(values, scales):
    square_mean = jnp.mean(values * values, axis=-1, keepdims=True)
    return values * lax.rsqrt(square_mean + epsilon) * scales


def rotate(values, positions):
    half_dim = values.shape[-1] // 2
    frequency = rotary_base ** (-jnp.arange(half_dim, dtype=jnp.float32) * 2.0 / values.shape[-1])
    angles = positions.astype(jnp.float32)[:, None] * frequency[None, :]
    layout = (values.shape[0],) + (1,) * (values.ndim - 2) + (half_dim,)
    cosine = jnp.cos(angles).reshape(layout)
    sine_table = jnp.sin(angles).reshape(layout)
    leading = values[..., :half_dim]
    trailing = values[..., half_dim:]
    return jnp.concatenate(
        [leading * cosine - trailing * sine_table, trailing * cosine + leading * sine_table],
        axis=-1,
    )


def attend_block(attention_state, key_rows, value_rows, key_pos, queries, query_pos):
    running_max, totals, weighted = attention_state
    scores = jnp.einsum("qhpd,khpd->hpqk", queries, key_rows, preferred_element_type=jnp.float32)
    visible = (key_pos[None, :] <= query_pos[:, None])[None, None, :, :]
    new_max = jnp.maximum(running_max, jnp.max(jnp.where(visible, scores, far_below), axis=-1))
    expo = jnp.where(visible, jnp.exp(scores - new_max[..., None]), 0.0)
    shrink = jnp.exp(running_max - new_max)
    totals = totals * shrink + jnp.sum(expo, axis=-1)
    weighted = weighted * shrink[..., None] + jnp.einsum(
        "hpqk,khe->hpqe", expo.astype(jnp.bfloat16), value_rows, preferred_element_type=jnp.float32
    )
    return (new_max, totals, weighted)


def fold_keys(attention_state, stacked, queries, query_pos, query_last):
    heads_here = queries.shape[1]
    head_size = queries.shape[3]
    number = stacked.shape[0]
    step_rows = math.gcd(number, 1024)
    key_cols = heads_here * 2 * head_size

    def one_block(block_index, running):
        row_begin = block_index * step_rows
        key_block = lax.dynamic_slice_in_dim(stacked, row_begin, step_rows, 0)
        key_rows = key_block[:, :key_cols].reshape(step_rows, heads_here, 2, head_size)
        value_rows = key_block[:, key_cols:].reshape(step_rows, heads_here, -1)
        key_pos = row_begin + jnp.arange(step_rows, dtype=jnp.int32)

        def update(unchanged):
            return attend_block(unchanged, key_rows, value_rows, key_pos, queries, query_pos)

        def keep(unchanged):
            return unchanged

        return lax.cond(jnp.min(key_pos) > query_last, keep, update, running)

    return lax.fori_loop(0, number // step_rows, one_block, attention_state)

MESH = pl.DeviceIdType.MESH
core_count = 2
weight_parts = 3
lane_count = 128


def greet(peers):
    barrier = pltpu.get_barrier_semaphore()
    for peer in peers:
        pl.semaphore_signal(barrier, inc=1, device_id=peer, device_id_type=MESH)
    pl.semaphore_wait(barrier, len(peers))


def places(planes):
    shard, column = lax.axis_index("ep"), lax.axis_index("tp")
    level, core = column // core_count, column % core_count

    def column_at(offset):
        return lax.rem(level + offset, planes) * core_count + core

    across_x = shard + 1 - 2 * lax.rem(shard, 2)
    across_y = lax.rem(shard + 2, 4)
    shards = (shard, across_x, across_y, lax.rem(across_x + 2, 4))
    return shards, column, core, column_at


def pushed(source, target, sems, index, peer):
    return pltpu.make_async_remote_copy(
        src_ref=source,
        dst_ref=target,
        send_sem=sems.at[(0,) + index],
        recv_sem=sems.at[(1,) + index],
        device_id=peer,
        device_id_type=MESH,
    )


def layer_kernel(
    planes, own, gate_in, up_in, down_in, queries, stacked, mix_in, lambdas, gain, out, mix_out,
    keyed, mix_weight, highest, totals, weighted, head_rows, mix_parts, mix_twins, mix_all,
    held, gate, up, down, parts, twins, x_part, y_part, x_all, y_all, z_all, kept,
    kv_sem, mp_sem, mz_sem, load_sem, az_sem, ax_sem, ay_sem, afx_sem, afy_sem, ap_sem,
    p_sem, fx_sem, fy_sem, x_sem, y_sem, z_sem,
):
    shards, column, core, column_at = places(planes)
    shard, across_x, across_y, across = shards
    other = 1 - core
    twin = (shard, column + 1 - 2 * core)
    x_peer, y_peer = (across_x, column), (across_y, column)
    rows, width = out.shape
    half = rows // 2
    wide = jnp.float32
    z_peers = {step: (shard, column_at(step)) for step in range(1, planes)}
    loads = [
        pltpu.make_async_copy(source, target, load_sem.at[at])
        for at, (source, target) in enumerate(
            [
                (own, held.at[0, 0, core]),
                (gate_in, gate),
                (up_in, up),
                (down_in, down),
                (mix_in, mix_weight),
                (stacked, keyed.at[0]),
            ]
        )
    ]
    for load in loads:
        load.start()
    greet([twin, x_peer, y_peer] + list(z_peers.values()))
    sent = []

    def push(*copy_parts):
        copy = pushed(*copy_parts)
        copy.start()
        sent.append(copy)

    def landed(block, sems, index):
        pushed(block, block, sems, index, twin).wait_recv()

    push(stacked, keyed.at[1], kv_sem, (0,), x_peer)
    push(stacked, keyed.at[2], kv_sem, (1,), y_peer)
    for step in range(1, planes):
        push(own, held.at[step, 0, core], az_sem, (step,), z_peers[step])

    def spread(step):
        block = held.at[step, 0, core]
        if step:
            landed(block, az_sem, (step,))
        source = block if step else own
        push(source, held.at[step, 1, core], ax_sem, (step,), x_peer)
        push(source, held.at[step, 2, core], ay_sem, (step,), y_peer)
        push(source, block, ap_sem, (step, 0), twin)

    def forward(step):
        across_block = held.at[step, 3, core]
        block = held.at[step, 1, core]
        landed(block, ax_sem, (step,))
        push(block.at[:half], across_block.at[:half], afy_sem, (step,), y_peer)
        push(block, block, ap_sem, (step, 1), twin)
        block = held.at[step, 2, core]
        landed(block, ay_sem, (step,))
        push(block.at[half:], across_block.at[half:], afx_sem, (step,), x_peer)
        push(block, block, ap_sem, (step, 2), twin)

    def finish(step):
        block = held.at[step, 3, core]
        landed(block.at[:half], afy_sem, (step,))
        landed(block.at[half:], afx_sem, (step,))
        push(block, block, ap_sem, (step, 3), twin)

    lane_expert = lax.broadcasted_iota(jnp.int32, (1, lane_count), 1) // weight_parts

    def compute(step):
        for which in range(4):
            landed(held.at[step, which, other], ap_sem, (step, which))

        def one_part(which, carry):
            block = held[step, which].reshape(core_count * rows, width + lane_count)
            lanes = jnp.where(lane_expert == shard, block[:, width:].astype(wide), 0.0)
            weights = jnp.sum(lanes, axis=1, keepdims=True)
            token_rows = block[:, :width]
            gate_act = jnp.dot(token_rows, gate[...], preferred_element_type=wide)
            upper = jnp.dot(token_rows, up[...], preferred_element_type=wide)
            hidden = (gate_act / (1.0 + jnp.exp(-gate_act)) * upper).astype(own.dtype)
            result = jnp.dot(hidden, down[...], preferred_element_type=wide)
            result = (result * weights).astype(own.dtype)
            parts[step, which] = result.reshape(core_count, rows, width)
            return carry

        lax.fori_loop(0, 4, one_part, 0)
        for which in (3, 1, 2, 0):
            push(parts.at[step, which, other], twins.at[step, which], p_sem, (step, which), twin)

    def pair(step, which):
        landed(twins.at[step, which], p_sem, (step, which))
        return parts[step, which, core].astype(wide) + twins[step, which].astype(wide)

    def narrow(values):
        return values.astype(own.dtype)

    def first(step):
        twins[step, 3] = narrow(pair(step, 3))
        push(twins.at[step, 3, :half], x_part.at[step], fx_sem, (step,), x_peer)
        push(twins.at[step, 3, half:], y_part.at[step], fy_sem, (step,), y_peer)

    def second(step):
        total = pair(step, 1)
        landed(y_part.at[step], fy_sem, (step,))
        twins[step, 1, :half] = narrow(total[:half])
        twins[step, 1, half:] = narrow(total[half:] + y_part[step].astype(wide))
        push(twins.at[step, 1], x_all.at[step], x_sem, (step,), x_peer)
        total = pair(step, 2)
        landed(x_part.at[step], fx_sem, (step,))
        twins[step, 2, :half] = narrow(total[:half] + x_part[step].astype(wide))
        twins[step, 2, half:] = narrow(total[half:])
        push(twins.at[step, 2], y_all.at[step], y_sem, (step,), y_peer)

    def third(step):
        total = pair(step, 0)
        landed(x_all.at[step], x_sem, (step,))
        landed(y_all.at[step], y_sem, (step,))
        total = total + x_all[step].astype(wide) + y_all[step].astype(wide)
        if step:
            twins[step, 0] = narrow(total)
            push(twins.at[step, 0], z_all.at[step], z_sem, (step,), z_peers[planes - step])
        else:
            kept[...] = total

    seq_rows, key_cols = keyed.shape[1], queries.shape[1] // 2
    heads_here = lambdas.shape[0]
    value_size = gain.shape[1]
    pair_size = key_cols // heads_here
    key_half = seq_rows // 2

    def attend(which, diagonal):
        for unit in range(2 * heads_here):
            head = unit // 2
            scores = lax.dot_general(
                queries[:, unit * pair_size : (unit + 1) * pair_size],
                keyed[which, :, head * pair_size : (head + 1) * pair_size],
                (((1,), (1,)), ((), ())),
                preferred_element_type=wide,
            )
            if diagonal:
                key_pos = lax.broadcasted_iota(jnp.int32, scores.shape, 1)
                query_pos = lax.broadcasted_iota(jnp.int32, scores.shape, 0)
                scores = jnp.where(key_pos <= query_pos, scores, far_below)
            top = jnp.max(scores, axis=1, keepdims=True)
            if not diagonal:
                top = jnp.maximum(top, highest[unit, :, :1])
            expo = jnp.exp(scores - top)
            total = jnp.sum(expo, axis=1, keepdims=True)
            first_col = key_cols + head * value_size
            value = jnp.dot(
                narrow(expo),
                keyed[which, :, first_col : first_col + value_size],
                preferred_element_type=wide,
            )
            if not diagonal:
                shrink = jnp.exp(highest[unit, :, :1] - top)
                total = total + totals[unit, :, :1] * shrink
                value = value + weighted[unit] * shrink
            highest[unit] = jnp.broadcast_to(top, highest.shape[1:])
            totals[unit] = jnp.broadcast_to(total, totals.shape[1:])
            weighted[unit] = value

    def attend_across(which, carry):
        across_shard = lax.rem(shard + which, 2) + 2 * lax.rem(shard // 2 + which // 2, 2)

        @pl.when(across_shard < shard)
        def _():
            attend(which, False)

        return carry

    def project():
        for head in range(heads_here):
            first_map = weighted[2 * head] / totals[2 * head]
            second_map = weighted[2 * head + 1] / totals[2 * head + 1]
            combined = first_map - lambdas[head : head + 1] * second_map
            cols = slice(head * value_size, (head + 1) * value_size)
            head_rows[:, cols] = narrow(norm_rows(combined, gain[...]))

        def one_plane(plane, carry):
            plane_rows = head_rows[pl.ds(plane * core_count * rows, core_count * rows), :]
            result = jnp.dot(plane_rows, mix_weight[...], preferred_element_type=wide)
            mix_parts[plane] = narrow(result).reshape(core_count, rows, width)
            return carry

        lax.fori_loop(0, planes, one_plane, 0)
        push(mix_parts.at[:, other], mix_twins, mp_sem, (0,), twin)

    level = column // core_count

    def mix_pair(step):
        plane = lax.rem(level + step, planes)
        return plane, mix_parts[plane, core].astype(wide) + mix_twins[plane].astype(wide)

    def mix_send():
        landed(mix_twins, mp_sem, (0,))
        for step in range(1, planes):
            plane, total = mix_pair(step)
            mix_twins[plane] = narrow(total)
            push(mix_twins.at[plane], mix_all.at[step], mz_sem, (step,), z_peers[step])

    def mix_finish():
        total = mix_pair(0)[1]
        for step in range(1, planes):
            landed(mix_all.at[step], mz_sem, (step,))
            total = total + mix_all[step].astype(wide)
        mix_out[...] = narrow(total)

    spread(0)
    for load in loads:
        load.wait()
    attend(0, True)
    landed(keyed.at[1], kv_sem, (0,))
    push(keyed.at[1, :key_half], keyed.at[3, :key_half], kv_sem, (2,), y_peer)
    landed(keyed.at[2], kv_sem, (1,))
    push(keyed.at[2, key_half:], keyed.at[3, key_half:], kv_sem, (3,), x_peer)
    for step in range(1, planes - 1):
        spread(step)
    landed(keyed.at[3, :key_half], kv_sem, (2,))
    landed(keyed.at[3, key_half:], kv_sem, (3,))
    lax.fori_loop(1, 4, attend_across, 0)
    project()
    spread(planes - 1)
    forward(0)
    mix_send()
    order = (forward, finish, first, compute, second, third)
    offset = (-1, 0, 1, 0, 1, 2)
    for at in range(planes + max(offset)):
        for stage, delay in zip(order, offset):
            if 0 <= at - delay < planes:
                stage(at - delay)
    mix_finish()
    total = kept[...]
    for step in range(1, planes):
        landed(z_all.at[step], z_sem, (step,))
        total = total + z_all[step].astype(wide)
    out[...] = narrow(total)
    for copy in sent:
        copy.wait_send()


def run_layer(
    payload, gate_weight, up_weight, down_weight, queries, stacked, mix_weight, lambdas, gain,
    column_count,
):
    planes = column_count // core_count
    rows = payload.shape[0]
    width = down_weight.shape[1]
    kind = payload.dtype

    def room(*sizes):
        return pltpu.VMEM(sizes, kind)

    one = pltpu.SemaphoreType.DMA((2, planes))
    four = pltpu.SemaphoreType.DMA((2, planes, 4))
    anywhere = pl.BlockSpec(memory_space=pl.ANY)
    near = pl.BlockSpec(memory_space=pltpu.VMEM)
    seq_rows = queries.shape[0]
    state = pltpu.VMEM((2 * lambdas.shape[0], seq_rows, gain.shape[1]), jnp.float32)
    return pl.pallas_call(
        lambda *refs: layer_kernel(planes, *refs),
        out_shape=[jax.ShapeDtypeStruct((rows, width), kind)] * 2,
        in_specs=[near, anywhere, anywhere, anywhere, near, near, anywhere, near, near],
        out_specs=[near, near],
        scratch_shapes=[
            room(4, *stacked.shape),
            room(*mix_weight.shape),
            state,
            state,
            state,
            room(seq_rows, mix_weight.shape[0]),
            room(planes, core_count, rows, width),
            room(planes, rows, width),
            room(planes, rows, width),
            room(planes, 4, core_count, rows, payload.shape[1]),
            room(*gate_weight.shape),
            room(*up_weight.shape),
            room(*down_weight.shape),
            room(planes, 4, core_count, rows, width),
            room(planes, 4, rows, width),
            room(planes, rows // 2, width),
            room(planes, rows // 2, width),
            room(planes, rows, width),
            room(planes, rows, width),
            room(planes, rows, width),
            pltpu.VMEM((rows, width), jnp.float32),
            pltpu.SemaphoreType.DMA((2, 4)),
            pltpu.SemaphoreType.DMA((2, 1)),
            one,
            pltpu.SemaphoreType.DMA((6,)),
            one, one, one, one, one, four, four, one, one, one, one, one,
        ],
        compiler_params=pltpu.CompilerParams(
            collective_id=0, has_side_effects=True, vmem_limit_bytes=62 * 1024 * 1024
        ),
        cost_estimate=pl.CostEstimate(flops=0, bytes_accessed=240000000, transcendentals=0),
        name="run_layer",
    )(
        payload, gate_weight, up_weight, down_weight, queries, stacked, mix_weight, lambdas, gain
    )


def token_payload(moe_input, moe_gain, expert_ids, route_weight):
    normed = norm_rows(moe_input.astype(jnp.float32), moe_gain).astype(jnp.bfloat16)
    lane_expert = jnp.arange(lane_count, dtype=jnp.int32) // weight_parts
    lane_part = jnp.arange(lane_count, dtype=jnp.int32) % weight_parts
    spread = jnp.sum(
        jnp.where(expert_ids[:, :, None] == lane_expert, route_weight[:, :, None], 0.0), axis=1
    )
    high = lax.reduce_precision(spread, 8, 7)
    middle = lax.reduce_precision(spread - high, 8, 7)
    low = spread - high - middle
    lanes = jnp.where(lane_part == 0, high, jnp.where(lane_part == 1, middle, low))
    return jnp.concatenate([normed, lanes.astype(jnp.bfloat16)], axis=1)


def experts_exchanged(
    moe_input, moe_gain, expert_ids, route_weight, gate_weight, up_weight, down_weight
):
    ep_size = lax.axis_size("ep")
    rows_b = moe_input.shape[0]
    top_count = expert_ids.shape[1]
    exp_here = gate_weight.shape[0]
    experts = exp_here * ep_size
    slot_count = 3 * rows_b * top_count // (2 * experts)
    normed = norm_rows(moe_input.astype(jnp.float32), moe_gain).astype(jnp.bfloat16)
    flat_ids = expert_ids.reshape(rows_b * top_count)
    member = (flat_ids[:, None] == jnp.arange(experts, dtype=jnp.int32)[None, :]).astype(jnp.int32)
    slot_rank = jnp.sum(member * (jnp.cumsum(member, axis=0) - 1), axis=1)
    target = (slot_rank * experts + flat_ids).reshape(rows_b, top_count)
    selector = (
        jnp.transpose(target)[:, :, None]
        == jnp.arange(slot_count * experts, dtype=jnp.int32)[None, None, :]
    ).astype(jnp.bfloat16)
    dispatched = jnp.einsum(
        "krs,rd->sd", selector, normed, preferred_element_type=jnp.float32
    ).astype(jnp.bfloat16)
    outgoing = dispatched.reshape(1, slot_count, experts, -1)
    arrived = lax.all_to_all(outgoing, "ep", split_axis=2, concat_axis=0, tiled=True)
    expert_rows = arrived.reshape(ep_size * slot_count, exp_here, -1)
    row_block = lax.all_gather(expert_rows, "tp", axis=0, tiled=True)
    gate_act = jnp.einsum(
        "mxd,xdf->mxf", row_block, gate_weight, preferred_element_type=jnp.float32
    )
    upper = jnp.einsum("mxd,xdf->mxf", row_block, up_weight, preferred_element_type=jnp.float32)
    hidden = (jax.nn.silu(gate_act) * upper).astype(jnp.bfloat16)
    row_block = hidden
    expert_sum = lax.psum_scatter(
        jnp.einsum(
            "mxf,xfd->mxd", row_block, down_weight, preferred_element_type=jnp.float32
        ).astype(jnp.bfloat16),
        "tp",
        scatter_dimension=0,
        tiled=True,
    )
    returning = expert_sum.reshape(ep_size, slot_count, exp_here, -1)
    returned = lax.all_to_all(returning, "ep", split_axis=0, concat_axis=2, tiled=True)
    results = returned.reshape(slot_count * experts, -1)
    chosen = jnp.einsum("krs,sd->krd", selector, results, preferred_element_type=jnp.float32)
    combined = jnp.sum(chosen * jnp.transpose(route_weight)[:, :, None], axis=0)
    return combined.astype(jnp.bfloat16)


def body(
    mix_query,
    mix_key,
    mix_value,
    head_lambda,
    head_gain,
    out_weight,
    moe_input,
    moe_gain,
    expert_ids,
    route_weight,
    gate_weight,
    up_weight,
    down_weight,
):
    seq_rows = mix_query.shape[0]
    heads_here = head_lambda.shape[0]
    head_size = mix_query.shape[1] // (2 * heads_here)
    value_size = mix_value.shape[1] // heads_here
    ep_size = lax.axis_size("ep")
    my_shard = lax.axis_index("ep")
    query_pos = my_shard * seq_rows + jnp.arange(seq_rows, dtype=jnp.int32)
    queries = rotate(
        mix_query.astype(jnp.float32).reshape(seq_rows, heads_here, 2, head_size), query_pos
    )
    queries = (queries * head_size ** (-0.5)).astype(jnp.bfloat16)
    rotated_keys = rotate(
        mix_key.astype(jnp.float32).reshape(seq_rows, heads_here, 2, head_size), query_pos
    )
    rotated_keys = rotated_keys.astype(jnp.bfloat16).reshape(seq_rows, heads_here * 2 * head_size)
    stacked = jnp.concatenate([rotated_keys, mix_value], axis=1)
    square = ep_size == 4 and lax.axis_size("tp") % core_count == 0
    if square and gate_weight.shape[0] == 1 and weight_parts * ep_size <= lane_count:
        map_of = jnp.eye(2, dtype=jnp.bfloat16)[None, None, :, :, None]
        apart = (queries[:, :, :, None, :] * map_of).reshape(seq_rows, -1)
        moe_output, mix_output = run_layer(
            token_payload(moe_input, moe_gain, expert_ids, route_weight),
            gate_weight[0],
            up_weight[0],
            down_weight[0],
            apart,
            stacked,
            out_weight,
            jnp.broadcast_to(head_lambda[:, None], (heads_here, value_size)),
            head_gain[None, :],
            lax.axis_size("tp"),
        )
        return (mix_output, moe_output)
    query_last = jnp.max(query_pos)
    initial = (
        jnp.full((heads_here, 2, seq_rows), far_below, jnp.float32),
        jnp.zeros((heads_here, 2, seq_rows), jnp.float32),
        jnp.zeros((heads_here, 2, seq_rows, value_size), jnp.float32),
    )
    attention_state = fold_keys(
        initial, lax.all_gather(stacked, "ep", axis=0, tiled=True), queries, query_pos, query_last
    )
    running_max, totals, weighted = attention_state
    lambdas = head_lambda[:, None, None]
    combined_heads = (
        weighted[:, 0] / totals[:, 0][..., None]
        - lambdas * weighted[:, 1] / totals[:, 1][..., None]
    )
    combined_heads = norm_rows(combined_heads, head_gain).astype(jnp.bfloat16)
    head_rows = jnp.transpose(combined_heads, (1, 0, 2)).reshape(seq_rows, heads_here * value_size)
    mix_partial = jnp.dot(head_rows, out_weight, preferred_element_type=jnp.float32)
    mix_sum = lax.psum_scatter(
        mix_partial.astype(jnp.bfloat16), "tp", scatter_dimension=0, tiled=True
    )
    moe_args = (
        moe_input, moe_gain, expert_ids, route_weight, gate_weight, up_weight, down_weight
    )
    return (mix_sum, experts_exchanged(*moe_args))


def solution(mesh):
    return jax.shard_map(
        body,
        mesh=mesh,
        in_specs=(
            P("ep", "tp"),
            P("ep", "tp"),
            P("ep", "tp"),
            P("tp"),
            P(),
            P("tp", None),
            P(("ep", "tp"), None),
            P(),
            P(("ep", "tp"), None),
            P(("ep", "tp"), None),
            P("ep", None, "tp"),
            P("ep", None, "tp"),
            P("ep", "tp", None),
        ),
        out_specs=(P(("ep", "tp"), None), P(("ep", "tp"), None)),
        check_vma=False,
    )
```

profile of v0, /device:TPU:0, one launch (start us, length us, event | category | flops | bytes accessed | tf_op | source)
XLA Modules:
  0.0 136.0 jit_solution(2453292609035822517)
XLA Ops:
  0.7 0.3 multiply_cosine_fusion
  1.0 1.1 copy.23
  2.1 0.1 convert.10
  2.1 1.1 copy.25
  3.2 0.1 convert.11
  3.3 0.1 subtract_convert_fusion
  3.4 0.0 copy-start.1
  3.6 0.0 copy-start.3
  3.6 0.0 copy-start.4
  3.6 0.0 copy-start
  3.6 0.0 copy-start.2
  3.6 0.2 copy.24
  3.8 0.0 copy-start.5
  3.9 0.1 copy.26
  4.0 0.1 mul.153
  4.1 0.1 mul.154
  4.2 0.2 copy-done.1
  4.4 1.1 pad_maximum_fusion
  5.5 0.0 copy-done.3
  5.5 0.0 copy-done.4
  5.5 0.1 select_reduce_fusion
  5.7 0.0 copy-done
  5.7 0.2 fusion
  5.8 0.0 copy-done.2
  5.8 0.1 fusion.2
  6.0 0.7 pad_maximum_fusion.1.refs_0_
  6.7 0.0 copy-done.5
  6.7 0.6 broadcast_in_dim.43.refs_7_
  7.3 125.4 %run_layer.1 = (bf16[64,2048]{1,0:T(8,128)(2,1)}, bf16[64,2048]{1,0:T(8,128)(2,1)}) custom-call(bf16[64,2176]{1,0:T(8,128)(2,1)} %pad_maximum_fusion.1.refs_0_, bf16[2048,512]{1,0:T(8,128)(2,1)} %bitcast.10, bf16[2048,512]{1,0:T(8,128)(2,1)} %bitcast.11, bf16[512,2048]{1,0:T(8,128)(2,1)} %bitcast.12, bf16[512,512]{1,0:T(8,128)(2,1)} %get-tuple-element.17.refs_4_, ...), custom_call_target="tpu_custom_call" | custom-call | bytes 240000000 | tf_op jit(solution)/shard_map/run_layer/pallas_call | solution.py:376
  132.7 1.7 %copy.29 = bf16[64,2048]{1,0:T(8,128)(2,1)} copy(bf16[64,2048]{1,0:T(8,128)(2,1)} %get-tuple-element.20) | data formatting | bytes 524288
  134.4 1.7 %copy.30 = bf16[64,2048]{1,0:T(8,128)(2,1)} copy(bf16[64,2048]{1,0:T(8,128)(2,1)} %get-tuple-element.21) | data formatting | bytes 524288
  (10 shorter events, 0.2 us)
Async XLA Ops:
  3.4 1.0 copy-start.1
  3.6 2.0 %copy-start.3 = (f32[64,2]{0,1:T(2,128)S(1)}, f32[64,2]{0,1:T(2,128)}, u32[]{:S(2)}) copy-start(f32[64,2]{0,1:T(2,128)} %param.22) | copy-start | bytes 1540
  3.6 2.0 %copy-start.4 = (s32[64,2]{0,1:T(2,128)S(1)}, s32[64,2]{0,1:T(2,128)}, u32[]{:S(2)}) copy-start(s32[64,2]{0,1:T(2,128)} %param.21) | copy-start | bytes 1540
  3.6 2.1 %copy-start = (bf16[64,2048]{1,0:T(8,128)(2,1)S(1)}, bf16[64,2048]{1,0:T(8,128)(2,1)}, u32[]{:S(2)}) copy-start(bf16[64,2048]{1,0:T(8,128)(2,1)} %param.19) | copy-start | bytes 786436
  3.6 2.2 %copy-start.2 = (f32[2048]{0:T(1024)S(1)}, f32[2048]{0:T(1024)}, u32[]{:S(2)}) copy-start(f32[2048]{0:T(1024)} %param.20) | copy-start | bytes 24580
  3.8 2.9 %copy-start.5 = (f32[2]{0:T(128)S(1)}, f32[2]{0:T(128)}, u32[]{:S(2)}) copy-start(f32[2]{0:T(128)} %param.16) | copy-start | bytes 28
where the time goes:
time: 136 us
  Pallas kernels  125 us (92%)
  local copies, waits for them, and re-layouts  6.96 us (5%)
  other arithmetic  2.88 us (2%)
    pallas_call x1, Pallas kernels, run_layer(): pl.pallas_call(lambda *refs: layer_kernel(planes, *refs), out_shape=[jax....  125 us
    unnamed x16, local copies, waits for them, and re-layouts  5.79 us

commit v1 on v0

--- a/solution.py
+++ b/solution.py
@@ -186,7 +186,8 @@
         for which in range(4):
             landed(held.at[step, which, other], ap_sem, (step, which))
 
-        def one_part(which, carry):
+        def one_part(turn, carry):
+            which = jnp.where(turn == 0, 3, jnp.where(turn == 3, 0, turn))
             block = held[step, which].reshape(core_count * rows, width + lane_count)
             lanes = jnp.where(lane_expert == shard, block[:, width:].astype(wide), 0.0)
             weights = jnp.sum(lanes, axis=1, keepdims=True)
@@ -197,11 +198,17 @@
             result = jnp.dot(hidden, down[...], preferred_element_type=wide)
             result = (result * weights).astype(own.dtype)
             parts[step, which] = result.reshape(core_count, rows, width)
+            part_copy(step, which).start()
             return carry
 
         lax.fori_loop(0, 4, one_part, 0)
-        for which in (3, 1, 2, 0):
-            push(parts.at[step, which, other], twins.at[step, which], p_sem, (step, which), twin)
+        for which in range(4):
+            sent.append(part_copy(step, which))
+
+    def part_copy(step, which):
+        return pushed(
+            parts.at[step, which, other], twins.at[step, which], p_sem, (step, which), twin
+        )
 
     def pair(step, which):
         landed(twins.at[step, which], p_sem, (step, which))
@@ -276,14 +283,12 @@
             totals[unit] = jnp.broadcast_to(total, totals.shape[1:])
             weighted[unit] = value
 
-    def attend_across(which, carry):
-        across_shard = lax.rem(shard + which, 2) + 2 * lax.rem(shard // 2 + which // 2, 2)
+    def attend_across(which):
+        across_shard = (shard, across_x, across_y, across)[which]
 
         @pl.when(across_shard < shard)
         def _():
             attend(which, False)
-
-        return carry
 
     def project():
         for head in range(heads_here):
@@ -323,28 +328,48 @@
         mix_out[...] = narrow(total)
 
     spread(0)
-    for load in loads:
-        load.wait()
+    loads[5].wait()
     attend(0, True)
+    spread(1)
+    forward(0)
     landed(keyed.at[1], kv_sem, (0,))
     push(keyed.at[1, :key_half], keyed.at[3, :key_half], kv_sem, (2,), y_peer)
     landed(keyed.at[2], kv_sem, (1,))
     push(keyed.at[2, key_half:], keyed.at[3, key_half:], kv_sem, (3,), x_peer)
-    for step in range(1, planes - 1):
-        spread(step)
+    spread(2)
+    attend_across(1)
+    attend_across(2)
+    forward(1)
+    spread(3)
+    finish(0)
+    for load in loads[:5]:
+        load.wait()
+    compute(0)
     landed(keyed.at[3, :key_half], kv_sem, (2,))
     landed(keyed.at[3, key_half:], kv_sem, (3,))
-    lax.fori_loop(1, 4, attend_across, 0)
+    attend_across(3)
     project()
-    spread(planes - 1)
-    forward(0)
+    forward(2)
     mix_send()
-    order = (forward, finish, first, compute, second, third)
-    offset = (-1, 0, 1, 0, 1, 2)
-    for at in range(planes + max(offset)):
-        for stage, delay in zip(order, offset):
-            if 0 <= at - delay < planes:
-                stage(at - delay)
+    finish(1)
+    compute(1)
+    forward(3)
+    first(1)
+    finish(2)
+    compute(2)
+    first(2)
+    first(0)
+    second(1)
+    finish(3)
+    compute(3)
+    first(3)
+    second(2)
+    third(1)
+    second(3)
+    third(2)
+    second(0)
+    third(3)
+    third(0)
     mix_finish()
     total = kept[...]
     for step in range(1, planes):

time: 136 us -> 121 us (0.89)
  Pallas kernels: 125 us -> 110 us
    pallas_call x1, Pallas kernels: 125 us -> 110 us  [run_layer(): pl.pallas_call(lambda *refs: layer_kernel(planes, *refs), out_shape=[jax....]
where the time goes in v1:
time: 121 us
  Pallas kernels  110 us (91%)
  local copies, waits for them, and re-layouts  6.96 us (6%)
  other arithmetic  2.88 us (2%)
    pallas_call x1, Pallas kernels, run_layer(): pl.pallas_call(lambda *refs: layer_kernel(planes, *refs), out_shape=[jax....  110 us
    unnamed x16, local copies, waits for them, and re-layouts  5.79 us

profile of v1, /device:TPU:0, one launch (start us, length us, event | category | flops | bytes accessed | tf_op | source)
XLA Modules:
  0.0 120.9 jit_solution(5319862184100440537)
XLA Ops:
  0.7 0.3 multiply_cosine_fusion
  1.0 1.1 copy.23
  2.1 0.1 convert.10
  2.1 1.1 copy.25
  3.2 0.1 convert.11
  3.3 0.1 subtract_convert_fusion
  3.4 0.0 copy-start.1
  3.6 0.0 copy-start.3
  3.6 0.0 copy-start.4
  3.6 0.0 copy-start
  3.6 0.0 copy-start.2
  3.6 0.2 copy.24
  3.8 0.0 copy-start.5
  3.9 0.1 copy.26
  4.0 0.1 mul.153
  4.1 0.1 mul.154
  4.2 0.2 copy-done.1
  4.4 1.1 pad_maximum_fusion
  5.5 0.0 copy-done.3
  5.5 0.0 copy-done.4
  5.5 0.1 select_reduce_fusion
  5.7 0.0 copy-done
  5.7 0.2 fusion
  5.8 0.0 copy-done.2
  5.8 0.1 fusion.2
  6.0 0.7 pad_maximum_fusion.1.refs_0_
  6.7 0.0 copy-done.5
  6.7 0.6 broadcast_in_dim.43.refs_7_
  7.3 110.2 %run_layer.1 = (bf16[64,2048]{1,0:T(8,128)(2,1)}, bf16[64,2048]{1,0:T(8,128)(2,1)}) custom-call(bf16[64,2176]{1,0:T(8,128)(2,1)} %pad_maximum_fusion.1.refs_0_, bf16[2048,512]{1,0:T(8,128)(2,1)} %bitcast.10, bf16[2048,512]{1,0:T(8,128)(2,1)} %bitcast.11, bf16[512,2048]{1,0:T(8,128)(2,1)} %bitcast.12, bf16[512,512]{1,0:T(8,128)(2,1)} %get-tuple-element.17.refs_4_, ...), custom_call_target="tpu_custom_call" | custom-call | bytes 240000000 | tf_op jit(solution)/shard_map/run_layer/pallas_call | solution.py:401
  117.6 1.7 %copy.29 = bf16[64,2048]{1,0:T(8,128)(2,1)} copy(bf16[64,2048]{1,0:T(8,128)(2,1)} %get-tuple-element.20) | data formatting | bytes 524288
  119.3 1.7 %copy.30 = bf16[64,2048]{1,0:T(8,128)(2,1)} copy(bf16[64,2048]{1,0:T(8,128)(2,1)} %get-tuple-element.21) | data formatting | bytes 524288
  (10 shorter events, 0.2 us)
Async XLA Ops:
  3.4 1.0 copy-start.1
  3.6 2.0 %copy-start.3 = (f32[64,2]{0,1:T(2,128)S(1)}, f32[64,2]{0,1:T(2,128)}, u32[]{:S(2)}) copy-start(f32[64,2]{0,1:T(2,128)} %param.22) | copy-start | bytes 1540
  3.6 2.0 %copy-start.4 = (s32[64,2]{0,1:T(2,128)S(1)}, s32[64,2]{0,1:T(2,128)}, u32[]{:S(2)}) copy-start(s32[64,2]{0,1:T(2,128)} %param.21) | copy-start | bytes 1540
  3.6 2.1 %copy-start = (bf16[64,2048]{1,0:T(8,128)(2,1)S(1)}, bf16[64,2048]{1,0:T(8,128)(2,1)}, u32[]{:S(2)}) copy-start(bf16[64,2048]{1,0:T(8,128)(2,1)} %param.19) | copy-start | bytes 786436
  3.6 2.2 %copy-start.2 = (f32[2048]{0:T(1024)S(1)}, f32[2048]{0:T(1024)}, u32[]{:S(2)}) copy-start(f32[2048]{0:T(1024)} %param.20) | copy-start | bytes 24580
  3.8 2.9 %copy-start.5 = (f32[2]{0:T(128)S(1)}, f32[2]{0:T(128)}, u32[]{:S(2)}) copy-start(f32[2]{0:T(128)} %param.16) | copy-start | bytes 28

commit v2 on v1

--- a/solution.py
+++ b/solution.py
@@ -2,6 +2,7 @@
 
 import jax
 import jax.numpy as jnp
+import numpy as np
 from jax import lax
 from jax.experimental import pallas as pl
 from jax.experimental.pallas import tpu as pltpu
@@ -87,8 +88,9 @@
     shard, column = lax.axis_index("ep"), lax.axis_index("tp")
     level, core = column // core_count, column % core_count
 
-    def column_at(offset):
-        return lax.rem(level + offset, planes) * core_count + core
+    def column_at(slot):
+        beside = level + 1 - 2 * lax.rem(level, 2)
+        return (level, beside, lax.rem(level + 2, planes), planes - 1 - level)[slot] * core_count + core
 
     across_x = shard + 1 - 2 * lax.rem(shard, 2)
     across_y = lax.rem(shard + 2, 4)
@@ -108,8 +110,10 @@
 
 
 def layer_kernel(
-    planes, own, gate_in, up_in, down_in, queries, stacked, mix_in, lambdas, gain, out, mix_out,
-    keyed, mix_weight, highest, totals, weighted, head_rows, mix_parts, mix_twins, mix_all,
+    planes, moe_in, moe_gain_in, ids_in, route_in, gate_in, up_in, down_in, query_in, key_in,
+    value_in, turn_in, mix_in, lambda_in, gain_in, out, mix_out,
+    moe_rows, moe_gain, ids, route, raw_query, raw_key, turns, lambdas, gain, queries,
+    cosines, sines, keyed, mix_weight, highest, totals, weighted, head_rows, mix_parts, mix_twins, mix_all,
     held, gate, up, down, parts, twins, x_part, y_part, x_all, y_all, z_all, kept,
     kv_sem, mp_sem, mz_sem, load_sem, az_sem, ax_sem, ay_sem, afx_sem, afy_sem, ap_sem,
     p_sem, fx_sem, fy_sem, x_sem, y_sem, z_sem,
@@ -122,23 +126,41 @@
     rows, width = out.shape
     half = rows // 2
     wide = jnp.float32
+    far_first = (2, 3, 1)
     z_peers = {step: (shard, column_at(step)) for step in range(1, planes)}
+    kind = held.dtype
+    key_cols = raw_key.shape[1]
     loads = [
         pltpu.make_async_copy(source, target, load_sem.at[at])
         for at, (source, target) in enumerate(
             [
-                (own, held.at[0, 0, core]),
+                (moe_in, moe_rows),
+                (moe_gain_in, moe_gain),
+                (ids_in, ids),
+                (route_in, route),
+                (key_in, raw_key),
+                (turn_in, turns),
+                (value_in, keyed.at[0, :, key_cols:]),
+                (query_in, raw_query),
                 (gate_in, gate),
                 (up_in, up),
                 (down_in, down),
                 (mix_in, mix_weight),
-                (stacked, keyed.at[0]),
+                (lambda_in, lambdas),
+                (gain_in, gain),
             ]
         )
     ]
     for load in loads:
         load.start()
-    greet([twin, x_peer, y_peer] + list(z_peers.values()))
+    peers = [twin, x_peer, y_peer] + list(z_peers.values())
+    barrier = pltpu.get_barrier_semaphore()
+    for peer in peers:
+        pl.semaphore_signal(barrier, inc=1, device_id=peer, device_id_type=MESH)
+    for load in loads[:4]:
+        load.wait()
+    held[0, 0, core] = token_payload(moe_rows[...], moe_gain[...], ids[...], route[...])
+    pl.semaphore_wait(barrier, len(peers))
     sent = []
 
     def push(*copy_parts):
@@ -149,19 +171,30 @@
     def landed(block, sems, index):
         pushed(block, block, sems, index, twin).wait_recv()
 
-    push(stacked, keyed.at[1], kv_sem, (0,), x_peer)
-    push(stacked, keyed.at[2], kv_sem, (1,), y_peer)
-    for step in range(1, planes):
-        push(own, held.at[step, 0, core], az_sem, (step,), z_peers[step])
+    def send_keys():
+        push(keyed.at[0], keyed.at[1], kv_sem, (0,), x_peer)
+        push(keyed.at[0], keyed.at[2], kv_sem, (1,), y_peer)
+
+    def send_planes():
+        for step in far_first:
+            push(held.at[0, 0, core], held.at[step, 0, core], az_sem, (step,), z_peers[step])
 
     def spread(step):
         block = held.at[step, 0, core]
         if step:
             landed(block, az_sem, (step,))
-        source = block if step else own
-        push(source, held.at[step, 1, core], ax_sem, (step,), x_peer)
-        push(source, held.at[step, 2, core], ay_sem, (step,), y_peer)
-        push(source, block, ap_sem, (step, 0), twin)
+        if step != 1:
+            push(block, held.at[step, 1, core], ax_sem, (step,), x_peer)
+            push(block, held.at[step, 2, core], ay_sem, (step,), y_peer)
+        push(block, block, ap_sem, (step, 0), twin)
+
+    def relay(which, sems):
+        push(held.at[0, which, core], held.at[1, which, core], sems, (1,), z_peers[1])
+
+    def gather(which, sems):
+        block = held.at[1, which, core]
+        landed(block, sems, (1,))
+        push(block, block, ap_sem, (1, which), twin)
 
     def forward(step):
         across_block = held.at[step, 3, core]
@@ -173,12 +206,17 @@
         landed(block, ay_sem, (step,))
         push(block.at[half:], across_block.at[half:], afx_sem, (step,), x_peer)
         push(block, block, ap_sem, (step, 2), twin)
+        if step == 0:
+            relay(1, ax_sem)
+            relay(2, ay_sem)
 
     def finish(step):
         block = held.at[step, 3, core]
         landed(block.at[:half], afy_sem, (step,))
         landed(block.at[half:], afx_sem, (step,))
         push(block, block, ap_sem, (step, 3), twin)
+        if step == 0:
+            relay(3, afx_sem)
 
     lane_expert = lax.broadcasted_iota(jnp.int32, (1, lane_count), 1) // weight_parts
 
@@ -194,9 +232,9 @@
             token_rows = block[:, :width]
             gate_act = jnp.dot(token_rows, gate[...], preferred_element_type=wide)
             upper = jnp.dot(token_rows, up[...], preferred_element_type=wide)
-            hidden = (gate_act / (1.0 + jnp.exp(-gate_act)) * upper).astype(own.dtype)
+            hidden = (gate_act / (1.0 + jnp.exp(-gate_act)) * upper).astype(kind)
             result = jnp.dot(hidden, down[...], preferred_element_type=wide)
-            result = (result * weights).astype(own.dtype)
+            result = (result * weights).astype(kind)
             parts[step, which] = result.reshape(core_count, rows, width)
             part_copy(step, which).start()
             return carry
@@ -215,7 +253,7 @@
         return parts[step, which, core].astype(wide) + twins[step, which].astype(wide)
 
     def narrow(values):
-        return values.astype(own.dtype)
+        return values.astype(kind)
 
     def first(step):
         twins[step, 3] = narrow(pair(step, 3))
@@ -241,15 +279,63 @@
         total = total + x_all[step].astype(wide) + y_all[step].astype(wide)
         if step:
             twins[step, 0] = narrow(total)
-            push(twins.at[step, 0], z_all.at[step], z_sem, (step,), z_peers[planes - step])
+            push(twins.at[step, 0], z_all.at[step], z_sem, (step,), z_peers[step])
         else:
             kept[...] = total
 
-    seq_rows, key_cols = keyed.shape[1], queries.shape[1] // 2
-    heads_here = lambdas.shape[0]
+    seq_rows = keyed.shape[1]
+    heads_here = lambdas.shape[1]
     value_size = gain.shape[1]
     pair_size = key_cols // heads_here
     key_half = seq_rows // 2
+
+    def wider(values):
+        return jnp.broadcast_to(values, (seq_rows, value_size))
+
+    turn_rows = seq_rows // 8
+    map_size = pair_size // 2
+    lane = lax.broadcasted_iota(jnp.int32, (turn_rows, pair_size), 1)
+    leading = lax.rem(lane, map_size) < map_size // 2
+
+    def rotated(source, rows_at, head, cosine, sine):
+        values = source[rows_at, head * pair_size : (head + 1) * pair_size].astype(wide)
+        ahead = pltpu.roll(values, pair_size - map_size // 2, 1)
+        behind = pltpu.roll(values, map_size // 2, 1)
+        return values * cosine + jnp.where(leading, ahead, behind) * sine
+
+    def rotate_keys():
+        def one_chunk(chunk, carry):
+            rows_at = pl.ds(pl.multiple_of(chunk * turn_rows, turn_rows), turn_rows)
+            place = lax.broadcasted_iota(jnp.int32, (turn_rows, pair_size), 0)
+            place = place + (shard * seq_rows + chunk * turn_rows)
+            angles = place.astype(wide) * turns[...]
+            cosine, sine = jnp.cos(angles), jnp.sin(angles)
+            sine = jnp.where(leading, -sine, sine)
+            cosines[rows_at, :] = cosine
+            sines[rows_at, :] = sine
+            for head in range(heads_here):
+                keyed[0, rows_at, head * pair_size : (head + 1) * pair_size] = narrow(
+                    rotated(raw_key, rows_at, head, cosine, sine)
+                )
+            return carry
+
+        lax.fori_loop(0, 8, one_chunk, 0)
+
+    def rotate_queries():
+        def one_chunk(chunk, carry):
+            rows_at = pl.ds(pl.multiple_of(chunk * turn_rows, turn_rows), turn_rows)
+            cosine, sine = cosines[rows_at, :], sines[rows_at, :]
+            for head in range(heads_here):
+                values = rotated(raw_query, rows_at, head, cosine, sine) * map_size ** (-0.5)
+                for half_at in range(2):
+                    unit = 2 * head + half_at
+                    own_map = (lane // map_size) == half_at
+                    queries[rows_at, unit * pair_size : (unit + 1) * pair_size] = narrow(
+                        jnp.where(own_map, values, 0.0)
+                    )
+            return carry
+
+        lax.fori_loop(0, 8, one_chunk, 0)
 
     def attend(which, diagonal):
         for unit in range(2 * heads_here):
@@ -264,11 +350,11 @@
                 key_pos = lax.broadcasted_iota(jnp.int32, scores.shape, 1)
                 query_pos = lax.broadcasted_iota(jnp.int32, scores.shape, 0)
                 scores = jnp.where(key_pos <= query_pos, scores, far_below)
-            top = jnp.max(scores, axis=1, keepdims=True)
+            top = wider(jnp.max(scores, axis=1, keepdims=True))
             if not diagonal:
-                top = jnp.maximum(top, highest[unit, :, :1])
-            expo = jnp.exp(scores - top)
-            total = jnp.sum(expo, axis=1, keepdims=True)
+                top = jnp.maximum(top, highest[unit])
+            expo = jnp.exp(scores - jnp.concatenate([top] * (seq_rows // value_size), axis=1))
+            total = wider(jnp.sum(expo, axis=1, keepdims=True))
             first_col = key_cols + head * value_size
             value = jnp.dot(
                 narrow(expo),
@@ -276,11 +362,11 @@
                 preferred_element_type=wide,
             )
             if not diagonal:
-                shrink = jnp.exp(highest[unit, :, :1] - top)
-                total = total + totals[unit, :, :1] * shrink
+                shrink = jnp.exp(highest[unit] - top)
+                total = total + totals[unit] * shrink
                 value = value + weighted[unit] * shrink
-            highest[unit] = jnp.broadcast_to(top, highest.shape[1:])
-            totals[unit] = jnp.broadcast_to(total, totals.shape[1:])
+            highest[unit] = top
+            totals[unit] = total
             weighted[unit] = value
 
     def attend_across(which):
@@ -294,7 +380,7 @@
         for head in range(heads_here):
             first_map = weighted[2 * head] / totals[2 * head]
             second_map = weighted[2 * head + 1] / totals[2 * head + 1]
-            combined = first_map - lambdas[head : head + 1] * second_map
+            combined = first_map - lambdas[:, head : head + 1] * second_map
             cols = slice(head * value_size, (head + 1) * value_size)
             head_rows[:, cols] = narrow(norm_rows(combined, gain[...]))
 
@@ -310,7 +396,7 @@
     level = column // core_count
 
     def mix_pair(step):
-        plane = lax.rem(level + step, planes)
+        plane = column_at(step) // core_count
         return plane, mix_parts[plane, core].astype(wide) + mix_twins[plane].astype(wide)
 
     def mix_send():
@@ -327,10 +413,14 @@
             total = total + mix_all[step].astype(wide)
         mix_out[...] = narrow(total)
 
+    send_planes()
     spread(0)
-    loads[5].wait()
+    for load in loads[4:8]:
+        load.wait()
+    rotate_keys()
+    send_keys()
+    rotate_queries()
     attend(0, True)
-    spread(1)
     forward(0)
     landed(keyed.at[1], kv_sem, (0,))
     push(keyed.at[1, :key_half], keyed.at[3, :key_half], kv_sem, (2,), y_peer)
@@ -339,10 +429,8 @@
     spread(2)
     attend_across(1)
     attend_across(2)
-    forward(1)
-    spread(3)
     finish(0)
-    for load in loads[:5]:
+    for load in loads[8:]:
         load.wait()
     compute(0)
     landed(keyed.at[3, :key_half], kv_sem, (2,))
@@ -350,25 +438,29 @@
     attend_across(3)
     project()
     forward(2)
+    spread(3)
+    spread(1)
     mix_send()
-    finish(1)
-    compute(1)
-    forward(3)
-    first(1)
     finish(2)
     compute(2)
     first(2)
+    gather(1, ax_sem)
+    forward(3)
     first(0)
-    second(1)
+    gather(2, ay_sem)
+    gather(3, afx_sem)
+    compute(1)
+    second(2)
     finish(3)
     compute(3)
     first(3)
-    second(2)
+    first(1)
+    third(2)
+    second(3)
+    second(1)
+    third(3)
+    second(0)
     third(1)
-    second(3)
-    third(2)
-    second(0)
-    third(3)
     third(0)
     mix_finish()
     total = kept[...]
@@ -381,13 +473,16 @@
 
 
 def run_layer(
-    payload, gate_weight, up_weight, down_weight, queries, stacked, mix_weight, lambdas, gain,
-    column_count,
+    moe_input, moe_gain, expert_ids, route_weight, gate_weight, up_weight, down_weight,
+    mix_query, mix_key, mix_value, turns, mix_weight, lambdas, gain, column_count,
 ):
     planes = column_count // core_count
-    rows = payload.shape[0]
-    width = down_weight.shape[1]
-    kind = payload.dtype
+    rows, width = moe_input.shape
+    kind = moe_input.dtype
+    arrays = [
+        moe_input, moe_gain, expert_ids, route_weight, gate_weight, up_weight, down_weight,
+        mix_query, mix_key, mix_value, turns, mix_weight, lambdas, gain,
+    ]
 
     def room(*sizes):
         return pltpu.VMEM(sizes, kind)
@@ -396,15 +491,31 @@
     four = pltpu.SemaphoreType.DMA((2, planes, 4))
     anywhere = pl.BlockSpec(memory_space=pl.ANY)
     near = pl.BlockSpec(memory_space=pltpu.VMEM)
-    seq_rows = queries.shape[0]
-    state = pltpu.VMEM((2 * lambdas.shape[0], seq_rows, gain.shape[1]), jnp.float32)
+    seq_rows, key_cols = mix_key.shape
+    state = pltpu.VMEM((2 * lambdas.shape[1], seq_rows, gain.shape[1]), jnp.float32)
+
+    def like(array):
+        return pltpu.VMEM(array.shape, array.dtype)
+
     return pl.pallas_call(
         lambda *refs: layer_kernel(planes, *refs),
-        out_shape=[jax.ShapeDtypeStruct((rows, width), kind)] * 2,
-        in_specs=[near, anywhere, anywhere, anywhere, near, near, anywhere, near, near],
+        out_shape=[pltpu.VMEM((rows, width), kind)] * 2,
+        in_specs=[anywhere] * len(arrays),
         out_specs=[near, near],
         scratch_shapes=[
-            room(4, *stacked.shape),
+            like(moe_input),
+            like(moe_gain),
+            like(expert_ids),
+            like(route_weight),
+            like(mix_query),
+            like(mix_key),
+            like(turns),
+            like(lambdas),
+            like(gain),
+            room(seq_rows, 2 * key_cols),
+            pltpu.VMEM((seq_rows, turns.shape[1]), jnp.float32),
+            pltpu.VMEM((seq_rows, turns.shape[1]), jnp.float32),
+            room(4, seq_rows, key_cols + mix_value.shape[1]),
             room(*mix_weight.shape),
             state,
             state,
@@ -413,7 +524,7 @@
             room(planes, core_count, rows, width),
             room(planes, rows, width),
             room(planes, rows, width),
-            room(planes, 4, core_count, rows, payload.shape[1]),
+            room(planes, 4, core_count, rows, width + lane_count),
             room(*gate_weight.shape),
             room(*up_weight.shape),
             room(*down_weight.shape),
@@ -428,7 +539,7 @@
             pltpu.SemaphoreType.DMA((2, 4)),
             pltpu.SemaphoreType.DMA((2, 1)),
             one,
-            pltpu.SemaphoreType.DMA((6,)),
+            pltpu.SemaphoreType.DMA((len(arrays),)),
             one, one, one, one, one, four, four, one, one, one, one, one,
         ],
         compiler_params=pltpu.CompilerParams(
@@ -436,23 +547,23 @@
         ),
         cost_estimate=pl.CostEstimate(flops=0, bytes_accessed=240000000, transcendentals=0),
         name="run_layer",
-    )(
-        payload, gate_weight, up_weight, down_weight, queries, stacked, mix_weight, lambdas, gain
-    )
-
-
-def token_payload(moe_input, moe_gain, expert_ids, route_weight):
-    normed = norm_rows(moe_input.astype(jnp.float32), moe_gain).astype(jnp.bfloat16)
-    lane_expert = jnp.arange(lane_count, dtype=jnp.int32) // weight_parts
-    lane_part = jnp.arange(lane_count, dtype=jnp.int32) % weight_parts
-    spread = jnp.sum(
-        jnp.where(expert_ids[:, :, None] == lane_expert, route_weight[:, :, None], 0.0), axis=1
-    )
-    high = lax.reduce_precision(spread, 8, 7)
-    middle = lax.reduce_precision(spread - high, 8, 7)
+    )(*arrays)
+
+
+def token_payload(moe_rows, moe_gain, expert_ids, route_weight):
+    kind = moe_rows.dtype
+    normed = norm_rows(moe_rows.astype(jnp.float32), moe_gain).astype(kind)
+    lane = lax.broadcasted_iota(jnp.int32, (lane_count, moe_rows.shape[0]), 0)
+    lane_expert, lane_part = lane // weight_parts, lax.rem(lane, weight_parts)
+    spread = jnp.zeros(lane.shape, jnp.float32)
+    for choice in range(expert_ids.shape[0]):
+        chosen = expert_ids[choice : choice + 1, :] == lane_expert
+        spread = spread + jnp.where(chosen, route_weight[choice : choice + 1, :], 0.0)
+    high = spread.astype(kind).astype(jnp.float32)
+    middle = (spread - high).astype(kind).astype(jnp.float32)
     low = spread - high - middle
     lanes = jnp.where(lane_part == 0, high, jnp.where(lane_part == 1, middle, low))
-    return jnp.concatenate([normed, lanes.astype(jnp.bfloat16)], axis=1)
+    return jnp.concatenate([normed, jnp.transpose(lanes).astype(kind)], axis=1)
 
 
 def experts_exchanged(
@@ -523,6 +634,28 @@
     value_size = mix_value.shape[1] // heads_here
     ep_size = lax.axis_size("ep")
     my_shard = lax.axis_index("ep")
+    tp_size = lax.axis_size("tp")
+    square = ep_size == 4 and tp_size == 4 * core_count
+    if square and gate_weight.shape[0] == 1 and weight_parts * ep_size <= lane_count:
+        frequency = rotary_base ** (-np.arange(head_size // 2) * 2.0 / head_size)
+        moe_output, mix_output = run_layer(
+            moe_input,
+            moe_gain[None, :],
+            jnp.transpose(expert_ids),
+            jnp.transpose(route_weight),
+            gate_weight[0],
+            up_weight[0],
+            down_weight[0],
+            mix_query,
+            mix_key,
+            mix_value,
+            jnp.asarray(np.tile(frequency, 4)[None, :], jnp.float32),
+            out_weight,
+            head_lambda[None, :],
+            head_gain[None, :],
+            tp_size,
+        )
+        return (mix_output, moe_output)
     query_pos = my_shard * seq_rows + jnp.arange(seq_rows, dtype=jnp.int32)
     queries = rotate(
         mix_query.astype(jnp.float32).reshape(seq_rows, heads_here, 2, head_size), query_pos
@@ -533,23 +666,6 @@
     )
     rotated_keys = rotated_keys.astype(jnp.bfloat16).reshape(seq_rows, heads_here * 2 * head_size)
     stacked = jnp.concatenate([rotated_keys, mix_value], axis=1)
-    square = ep_size == 4 and lax.axis_size("tp") % core_count == 0
-    if square and gate_weight.shape[0] == 1 and weight_parts * ep_size <= lane_count:
-        map_of = jnp.eye(2, dtype=jnp.bfloat16)[None, None, :, :, None]
-        apart = (queries[:, :, :, None, :] * map_of).reshape(seq_rows, -1)
-        moe_output, mix_output = run_layer(
-            token_payload(moe_input, moe_gain, expert_ids, route_weight),
-            gate_weight[0],
-            up_weight[0],
-            down_weight[0],
-            apart,
-            stacked,
-            out_weight,
-            jnp.broadcast_to(head_lambda[:, None], (heads_here, value_size)),
-            head_gain[None, :],
-            lax.axis_size("tp"),
-        )
-        return (mix_output, moe_output)
     query_last = jnp.max(query_pos)
     initial = (
         jnp.full((heads_here, 2, seq_rows), far_below, jnp.float32),

time: 121 us -> 95.4 us (0.79)
  Pallas kernels: 110 us -> 93.2 us
  local copies, waits for them, and re-layouts: 6.96 us -> 1.41 us
  other arithmetic: 2.88 us -> 0 us
    pallas_call x1, Pallas kernels: 110 us -> 93.2 us  [run_layer(): pl.pallas_call(lambda *refs: layer_kernel(planes, *refs), out_shape=[pltp...]
    unnamed x16 -> x2, local copies, waits for them, and re-layouts: 5.79 us -> 1.41 us
    concatenate x3 -> x0, other arithmetic: 1.84 us -> none  [the longest x1 1.09 us: body(): stacked = jnp.concatenate([rotated_keys, mix_value], axis=1)]
where the time goes in v2:
time: 95.4 us; the launch traced here: 95.3 us
  Pallas kernels  93.2 us (98%)
  local copies, waits for them, and re-layouts  1.41 us (1%)
    pallas_call x1, Pallas kernels, run_layer(): pl.pallas_call(lambda *refs: layer_kernel(planes, *refs), out_shape=[pltp...  93.2 us

profile of v2, /device:TPU:0, one launch (start us, length us, event | category | flops | bytes accessed | tf_op | source)
XLA Modules:
  0.0 95.3 jit_solution(10289482291131063949)
XLA Ops:
  0.6 93.2 %run_layer.1 = (bf16[64,2048]{1,0:T(8,128)(2,1)S(1)}, bf16[64,2048]{1,0:T(8,128)(2,1)S(1)}) custom-call(bf16[64,2048]{1,0:T(8,128)(2,1)} %refs_0_.1, f32[1,2048]{1,0:T(1,128)} %bitcast.11, s32[2,64]{1,0:T(2,128)} %bitcast.12, f32[2,64]{1,0:T(2,128)} %bitcast.13, bf16[2048,512]{1,0:T(8,128)(2,1)} %bitcast.8, bf16[2048,512]{1,0:T(8,128)(2,1)} %bitcast.9, ...), custom_call_target="tpu_custom_call" | custom-call | bytes 240000000 | tf_op jit(solution)/shard_map/run_layer/pallas_call | solution.py:500
  93.9 0.7 copy.18
  94.6 0.7 copy.19

commit v3 on v2

--- a/solution.py
+++ b/solution.py
@@ -184,31 +184,45 @@
         if step:
             landed(block, az_sem, (step,))
         if step != 1:
-            push(block, held.at[step, 1, core], ax_sem, (step,), x_peer)
-            push(block, held.at[step, 2, core], ay_sem, (step,), y_peer)
+            for turn, (part, late) in enumerate((("low", "high"), ("high", "low"))):
+                for sems, which, peer, name in (
+                    (ax_sem, 1, x_peer, part),
+                    (ay_sem, 2, y_peer, late),
+                ):
+                    target = held.at[step, which, core]
+                    push(cut(block, name), cut(target, name), sems, (step, turn), peer)
         push(block, block, ap_sem, (step, 0), twin)
 
-    def relay(which, sems):
-        push(held.at[0, which, core], held.at[1, which, core], sems, (1,), z_peers[1])
-
-    def gather(which, sems):
+    def cut(block, name):
+        return block.at[:half] if name == "low" else block.at[half:]
+
+    def relay(which, sems, index):
+        push(held.at[0, which, core], held.at[1, which, core], sems, index, z_peers[1])
+
+    def gather(which, sems, index):
         block = held.at[1, which, core]
-        landed(block, sems, (1,))
+        landed(block, sems, index)
         push(block, block, ap_sem, (1, which), twin)
 
     def forward(step):
         across_block = held.at[step, 3, core]
         block = held.at[step, 1, core]
-        landed(block, ax_sem, (step,))
+        landed(block.at[:half], ax_sem, (step, 0))
         push(block.at[:half], across_block.at[:half], afy_sem, (step,), y_peer)
+        block = held.at[step, 2, core]
+        landed(block.at[half:], ay_sem, (step, 0))
+        push(block.at[half:], across_block.at[half:], afx_sem, (step,), x_peer)
+
+    def settle(step):
+        block = held.at[step, 1, core]
+        landed(block.at[half:], ax_sem, (step, 1))
         push(block, block, ap_sem, (step, 1), twin)
         block = held.at[step, 2, core]
-        landed(block, ay_sem, (step,))
-        push(block.at[half:], across_block.at[half:], afx_sem, (step,), x_peer)
+        landed(block.at[:half], ay_sem, (step, 1))
         push(block, block, ap_sem, (step, 2), twin)
         if step == 0:
-            relay(1, ax_sem)
-            relay(2, ay_sem)
+            relay(1, ax_sem, (1, 0))
+            relay(2, ay_sem, (1, 0))
 
     def finish(step):
         block = held.at[step, 3, core]
@@ -216,7 +230,7 @@
         landed(block.at[half:], afx_sem, (step,))
         push(block, block, ap_sem, (step, 3), twin)
         if step == 0:
-            relay(3, afx_sem)
+            relay(3, afx_sem, (1,))
 
     lane_expert = lax.broadcasted_iota(jnp.int32, (1, lane_count), 1) // weight_parts
 
@@ -248,9 +262,13 @@
             parts.at[step, which, other], twins.at[step, which], p_sem, (step, which), twin
         )
 
+    def sums(step, which, begin, end):
+        mine = parts[step, which, core, begin:end].astype(wide)
+        return mine + twins[step, which, begin:end].astype(wide)
+
     def pair(step, which):
         landed(twins.at[step, which], p_sem, (step, which))
-        return parts[step, which, core].astype(wide) + twins[step, which].astype(wide)
+        return sums(step, which, 0, rows)
 
     def narrow(values):
         return values.astype(kind)
@@ -260,22 +278,29 @@
         push(twins.at[step, 3, :half], x_part.at[step], fx_sem, (step,), x_peer)
         push(twins.at[step, 3, half:], y_part.at[step], fy_sem, (step,), y_peer)
 
+    def early(step):
+        for which in (1, 2):
+            landed(twins.at[step, which], p_sem, (step, which))
+        twins[step, 1, :half] = narrow(sums(step, 1, 0, half))
+        push(twins.at[step, 1, :half], x_all.at[step, :half], x_sem, (step, 0), x_peer)
+        twins[step, 2, half:] = narrow(sums(step, 2, half, rows))
+        push(twins.at[step, 2, half:], y_all.at[step, half:], y_sem, (step, 0), y_peer)
+
     def second(step):
-        total = pair(step, 1)
+        total = sums(step, 1, half, rows)
         landed(y_part.at[step], fy_sem, (step,))
-        twins[step, 1, :half] = narrow(total[:half])
-        twins[step, 1, half:] = narrow(total[half:] + y_part[step].astype(wide))
-        push(twins.at[step, 1], x_all.at[step], x_sem, (step,), x_peer)
-        total = pair(step, 2)
+        twins[step, 1, half:] = narrow(total + y_part[step].astype(wide))
+        push(twins.at[step, 1, half:], x_all.at[step, half:], x_sem, (step, 1), x_peer)
+        total = sums(step, 2, 0, half)
         landed(x_part.at[step], fx_sem, (step,))
-        twins[step, 2, :half] = narrow(total[:half] + x_part[step].astype(wide))
-        twins[step, 2, half:] = narrow(total[half:])
-        push(twins.at[step, 2], y_all.at[step], y_sem, (step,), y_peer)
+        twins[step, 2, :half] = narrow(total + x_part[step].astype(wide))
+        push(twins.at[step, 2, :half], y_all.at[step, :half], y_sem, (step, 1), y_peer)
 
     def third(step):
         total = pair(step, 0)
-        landed(x_all.at[step], x_sem, (step,))
-        landed(y_all.at[step], y_sem, (step,))
+        for part in range(2):
+            landed(x_all.at[step, part * half : (part + 1) * half], x_sem, (step, part))
+            landed(y_all.at[step, (1 - part) * half : (2 - part) * half], y_sem, (step, part))
         total = total + x_all[step].astype(wide) + y_all[step].astype(wide)
         if step:
             twins[step, 0] = narrow(total)
@@ -422,45 +447,52 @@
     rotate_queries()
     attend(0, True)
     forward(0)
+    settle(0)
     landed(keyed.at[1], kv_sem, (0,))
     push(keyed.at[1, :key_half], keyed.at[3, :key_half], kv_sem, (2,), y_peer)
     landed(keyed.at[2], kv_sem, (1,))
     push(keyed.at[2, key_half:], keyed.at[3, key_half:], kv_sem, (3,), x_peer)
+    finish(0)
     spread(2)
     attend_across(1)
     attend_across(2)
-    finish(0)
-    for load in loads[8:]:
-        load.wait()
-    compute(0)
     landed(keyed.at[3, :key_half], kv_sem, (2,))
     landed(keyed.at[3, key_half:], kv_sem, (3,))
     attend_across(3)
+    for load in loads[8:]:
+        load.wait()
     project()
     forward(2)
+    mix_send()
+    gather(1, ax_sem, (1, 0))
+    settle(2)
     spread(3)
-    spread(1)
-    mix_send()
     finish(2)
+    forward(3)
     compute(2)
     first(2)
-    gather(1, ax_sem)
-    forward(3)
-    first(0)
-    gather(2, ay_sem)
-    gather(3, afx_sem)
-    compute(1)
+    finish(3)
+    spread(1)
+    gather(2, ay_sem, (1, 0))
+    early(2)
+    settle(3)
+    gather(3, afx_sem, (1,))
     second(2)
-    finish(3)
     compute(3)
     first(3)
+    early(3)
+    third(2)
+    compute(1)
     first(1)
-    third(2)
     second(3)
+    compute(0)
+    early(1)
+    third(3)
     second(1)
-    third(3)
+    first(0)
+    early(0)
+    third(1)
     second(0)
-    third(1)
     third(0)
     mix_finish()
     total = kept[...]
@@ -488,6 +520,7 @@
         return pltpu.VMEM(sizes, kind)
 
     one = pltpu.SemaphoreType.DMA((2, planes))
+    two = pltpu.SemaphoreType.DMA((2, planes, 2))
     four = pltpu.SemaphoreType.DMA((2, planes, 4))
     anywhere = pl.BlockSpec(memory_space=pl.ANY)
     near = pl.BlockSpec(memory_space=pltpu.VMEM)
@@ -540,7 +573,7 @@
             pltpu.SemaphoreType.DMA((2, 1)),
             one,
             pltpu.SemaphoreType.DMA((len(arrays),)),
-            one, one, one, one, one, four, four, one, one, one, one, one,
+            one, two, two, one, one, four, four, one, one, two, two, one,
         ],
         compiler_params=pltpu.CompilerParams(
             collective_id=0, has_side_effects=True, vmem_limit_bytes=62 * 1024 * 1024

time: 95.4 us -> 92.1 us (0.965)
  Pallas kernels: 93.2 us -> 89.9 us
    pallas_call x1, Pallas kernels: 93.2 us -> 89.9 us  [run_layer(): pl.pallas_call(lambda *refs: layer_kernel(planes, *refs), out_shape=[pltp...]
where the time goes in v3:
time: 92.1 us; the launch traced here: 91.9 us
  Pallas kernels  89.9 us (98%)
  local copies, waits for them, and re-layouts  1.41 us (2%)
    pallas_call x1, Pallas kernels, run_layer(): pl.pallas_call(lambda *refs: layer_kernel(planes, *refs), out_shape=[pltp...  89.9 us

profile of v3, /device:TPU:0, one launch (start us, length us, event | category | flops | bytes accessed | tf_op | source)
XLA Modules:
  0.0 91.9 jit_solution(16554057114746441436)
XLA Ops:
  0.6 89.9 %run_layer.1 = (bf16[64,2048]{1,0:T(8,128)(2,1)S(1)}, bf16[64,2048]{1,0:T(8,128)(2,1)S(1)}) custom-call(bf16[64,2048]{1,0:T(8,128)(2,1)} %refs_0_.1, f32[1,2048]{1,0:T(1,128)} %bitcast.11, s32[2,64]{1,0:T(2,128)} %bitcast.12, f32[2,64]{1,0:T(2,128)} %bitcast.13, bf16[2048,512]{1,0:T(8,128)(2,1)} %bitcast.8, bf16[2048,512]{1,0:T(8,128)(2,1)} %bitcast.9, ...), custom_call_target="tpu_custom_call" | custom-call | bytes 240000000 | tf_op jit(solution)/shard_map/run_layer/pallas_call | solution.py:533
  90.5 0.7 copy.18
  91.2 0.7 copy.19

commit v4 on v3

--- a/solution.py
+++ b/solution.py
@@ -73,8 +73,7 @@
 
 MESH = pl.DeviceIdType.MESH
 core_count = 2
-weight_parts = 3
-lane_count = 128
+share_rows = 8
 
 
 def greet(peers):
@@ -114,7 +113,7 @@
     value_in, turn_in, mix_in, lambda_in, gain_in, out, mix_out,
     moe_rows, moe_gain, ids, route, raw_query, raw_key, turns, lambdas, gain, queries,
     cosines, sines, keyed, mix_weight, highest, totals, weighted, head_rows, mix_parts, mix_twins, mix_all,
-    held, gate, up, down, parts, twins, x_part, y_part, x_all, y_all, z_all, kept,
+    held, gate, up, down, parts, twins, x_part, y_part, x_all, y_all, z_all, kept, shares, wz_sem, ws_sem,
     kv_sem, mp_sem, mz_sem, load_sem, az_sem, ax_sem, ay_sem, afx_sem, afy_sem, ap_sem,
     p_sem, fx_sem, fy_sem, x_sem, y_sem, z_sem,
 ):
@@ -159,7 +158,8 @@
         pl.semaphore_signal(barrier, inc=1, device_id=peer, device_id_type=MESH)
     for load in loads[:4]:
         load.wait()
-    held[0, 0, core] = token_payload(moe_rows[...], moe_gain[...], ids[...], route[...])
+    held[0, 0, core] = norm_rows(moe_rows[...].astype(wide), moe_gain[...]).astype(kind)
+    shares[0, 0, core] = route_shares(ids[...], route[...], core)
     pl.semaphore_wait(barrier, len(peers))
     sent = []
 
@@ -232,7 +232,36 @@
         if step == 0:
             relay(3, afx_sem, (1,))
 
-    lane_expert = lax.broadcasted_iota(jnp.int32, (1, lane_count), 1) // weight_parts
+    token_count = core_count * rows
+
+    def share_planes():
+        block = shares.at[0, 0, core]
+        for step in (1, 2, 3):
+            push(block, shares.at[step, 0, core], wz_sem, (step,), z_peers[step])
+
+    def share_sides():
+        for step in (1, 2, 3):
+            landed(shares.at[step, 0, core], wz_sem, (step,))
+        push(shares.at[:, 0, core], shares.at[:, 1, core], ws_sem, (0,), x_peer)
+        push(shares.at[:, 0, core], shares.at[:, 2, core], ws_sem, (1,), y_peer)
+
+    def share_across():
+        landed(shares.at[:, 1, core], ws_sem, (0,))
+        push(shares.at[:, 1, core], shares.at[:, 3, core], ws_sem, (2,), y_peer)
+
+    def share_twin():
+        landed(shares.at[:, 2, core], ws_sem, (1,))
+        landed(shares.at[:, 3, core], ws_sem, (2,))
+        push(shares.at[:, :, core], shares.at[:, :, core], ws_sem, (3,), twin)
+
+    def share_column(step, which):
+        share = shares[step, which, 0]
+        for place in range(1, core_count):
+            share = share + shares[step, which, place]
+        expert = lax.broadcasted_iota(jnp.int32, share.shape, 0)
+        row = jnp.sum(jnp.where(expert == shard, share, 0.0), axis=0, keepdims=True)
+        column = jnp.transpose(jnp.broadcast_to(row, (token_count, token_count)))
+        return jnp.concatenate([column] * (width // token_count), axis=1)
 
     def compute(step):
         for which in range(4):
@@ -240,15 +269,12 @@
 
         def one_part(turn, carry):
             which = jnp.where(turn == 0, 3, jnp.where(turn == 3, 0, turn))
-            block = held[step, which].reshape(core_count * rows, width + lane_count)
-            lanes = jnp.where(lane_expert == shard, block[:, width:].astype(wide), 0.0)
-            weights = jnp.sum(lanes, axis=1, keepdims=True)
-            token_rows = block[:, :width]
+            token_rows = held[step, which].reshape(token_count, width)
             gate_act = jnp.dot(token_rows, gate[...], preferred_element_type=wide)
             upper = jnp.dot(token_rows, up[...], preferred_element_type=wide)
             hidden = (gate_act / (1.0 + jnp.exp(-gate_act)) * upper).astype(kind)
             result = jnp.dot(hidden, down[...], preferred_element_type=wide)
-            result = (result * weights).astype(kind)
+            result = (result * share_column(step, which)).astype(kind)
             parts[step, which] = result.reshape(core_count, rows, width)
             part_copy(step, which).start()
             return carry
@@ -438,6 +464,7 @@
             total = total + mix_all[step].astype(wide)
         mix_out[...] = narrow(total)
 
+    share_planes()
     send_planes()
     spread(0)
     for load in loads[4:8]:
@@ -446,8 +473,10 @@
     send_keys()
     rotate_queries()
     attend(0, True)
+    share_sides()
     forward(0)
     settle(0)
+    share_across()
     landed(keyed.at[1], kv_sem, (0,))
     push(keyed.at[1, :key_half], keyed.at[3, :key_half], kv_sem, (2,), y_peer)
     landed(keyed.at[2], kv_sem, (1,))
@@ -456,6 +485,7 @@
     spread(2)
     attend_across(1)
     attend_across(2)
+    share_twin()
     landed(keyed.at[3, :key_half], kv_sem, (2,))
     landed(keyed.at[3, key_half:], kv_sem, (3,))
     attend_across(3)
@@ -469,6 +499,7 @@
     spread(3)
     finish(2)
     forward(3)
+    landed(shares.at[:, :, other], ws_sem, (3,))
     compute(2)
     first(2)
     finish(3)
@@ -493,8 +524,8 @@
     early(0)
     third(1)
     second(0)
+    mix_finish()
     third(0)
-    mix_finish()
     total = kept[...]
     for step in range(1, planes):
         landed(z_all.at[step], z_sem, (step,))
@@ -557,7 +588,7 @@
             room(planes, core_count, rows, width),
             room(planes, rows, width),
             room(planes, rows, width),
-            room(planes, 4, core_count, rows, width + lane_count),
+            room(planes, 4, core_count, rows, width),
             room(*gate_weight.shape),
             room(*up_weight.shape),
             room(*down_weight.shape),
@@ -569,6 +600,9 @@
             room(planes, rows, width),
             room(planes, rows, width),
             pltpu.VMEM((rows, width), jnp.float32),
+            pltpu.VMEM((planes, 4, core_count, share_rows, core_count * rows), jnp.float32),
+            one,
+            one,
             pltpu.SemaphoreType.DMA((2, 4)),
             pltpu.SemaphoreType.DMA((2, 1)),
             one,
@@ -583,20 +617,17 @@
     )(*arrays)
 
 
-def token_payload(moe_rows, moe_gain, expert_ids, route_weight):
-    kind = moe_rows.dtype
-    normed = norm_rows(moe_rows.astype(jnp.float32), moe_gain).astype(kind)
-    lane = lax.broadcasted_iota(jnp.int32, (lane_count, moe_rows.shape[0]), 0)
-    lane_expert, lane_part = lane // weight_parts, lax.rem(lane, weight_parts)
-    spread = jnp.zeros(lane.shape, jnp.float32)
-    for choice in range(expert_ids.shape[0]):
-        chosen = expert_ids[choice : choice + 1, :] == lane_expert
-        spread = spread + jnp.where(chosen, route_weight[choice : choice + 1, :], 0.0)
-    high = spread.astype(kind).astype(jnp.float32)
-    middle = (spread - high).astype(kind).astype(jnp.float32)
-    low = spread - high - middle
-    lanes = jnp.where(lane_part == 0, high, jnp.where(lane_part == 1, middle, low))
-    return jnp.concatenate([normed, jnp.transpose(lanes).astype(kind)], axis=1)
+def route_shares(expert_ids, route_weight, core):
+    choices, rows = expert_ids.shape
+    expert = lax.broadcasted_iota(jnp.int32, (share_rows, rows), 0)
+    share = jnp.zeros(expert.shape, jnp.float32)
+    for choice in range(choices):
+        chosen = expert_ids[choice : choice + 1, :] == expert
+        share = share + jnp.where(chosen, route_weight[choice : choice + 1, :], 0.0)
+    empty = jnp.zeros_like(share)
+    return jnp.concatenate(
+        [jnp.where(core == place, share, empty) for place in range(core_count)], axis=1
+    )
 
 
 def experts_exchanged(
@@ -669,7 +700,7 @@
     my_shard = lax.axis_index("ep")
     tp_size = lax.axis_size("tp")
     square = ep_size == 4 and tp_size == 4 * core_count
-    if square and gate_weight.shape[0] == 1 and weight_parts * ep_size <= lane_count:
+    if square and gate_weight.shape[0] == 1 and ep_size <= share_rows:
         frequency = rotary_base ** (-np.arange(head_size // 2) * 2.0 / head_size)
         moe_output, mix_output = run_layer(
             moe_input,

time: 92.1 us -> 91.6 us (level)
  no operation moved by 1% of the time
where the time goes in v4:
time: 91.6 us; the launch traced here: 91.4 us
  Pallas kernels  89.4 us (98%)
  local copies, waits for them, and re-layouts  1.41 us (2%)
    pallas_call x1, Pallas kernels, run_layer(): pl.pallas_call(lambda *refs: layer_kernel(planes, *refs), out_shape=[pltp...  89.4 us

profile of v4, /device:TPU:0, one launch (start us, length us, event | category | flops | bytes accessed | tf_op | source)
XLA Modules:
  0.0 91.4 jit_solution(10683865782308645158)
XLA Ops:
  0.6 89.4 %run_layer.1 = (bf16[64,2048]{1,0:T(8,128)(2,1)S(1)}, bf16[64,2048]{1,0:T(8,128)(2,1)S(1)}) custom-call(bf16[64,2048]{1,0:T(8,128)(2,1)} %refs_0_.1, f32[1,2048]{1,0:T(1,128)} %bitcast.11, s32[2,64]{1,0:T(2,128)} %bitcast.12, f32[2,64]{1,0:T(2,128)} %bitcast.13, bf16[2048,512]{1,0:T(8,128)(2,1)} %bitcast.8, bf16[2048,512]{1,0:T(8,128)(2,1)} %bitcast.9, ...), custom_call_target="tpu_custom_call" | custom-call | bytes 240000000 | tf_op jit(solution)/shard_map/run_layer/pallas_call | solution.py:564
  90.0 0.7 copy.18
  90.7 0.7 copy.19
